TPU v7x, 256 devices: a whole 4x4x8 slice. The times are simulated.
256 devices in a mesh: dp: 4 (over y), kv: 32 (over z, x), tp: 2 (over core).
Axes of the slice: x: 4, y: 4, z: 8, core: 2. Of those that a mesh axis runs over, the one named last changes fastest.
Arguments:
- tokens: bfloat16 [16, 4096], P('dp', 'kv'), may hold values from -18 to 18
- norm_gain: float32 [4096], P('kv'), may hold values from 0.1 to 1.9
- query_weight: bfloat16 [4096, 4096], P('kv', 'tp'), may hold values from -0.09375 to 0.09375
- key_weight: bfloat16 [4096, 512], P('kv', 'tp'), may hold values from -0.09375 to 0.09375
- value_weight: bfloat16 [4096, 512], P('kv', 'tp'), may hold values from -0.09375 to 0.09375
- gate_weight: bfloat16 [4096, 8], replicated, may hold values from -0.09375 to 0.09375
- gate_bias: float32 [8], replicated, may hold values from -2.5 to 0.5
- query_gain: float32 [64], replicated, may hold values from 0.1 to 1.9
- key_gain: float32 [64], replicated, may hold values from 0.1 to 1.9
- key_cache: bfloat16 [16, 65536, 512], P('dp', 'kv', 'tp'), may hold values from -6 to 6
- value_cache: bfloat16 [16, 65536, 512], P('dp', 'kv', 'tp'), may hold values from -9 to 9
- gate_cache: float32 [16, 8, 65536], P('dp', 'tp', 'kv'), may hold values from -65536 to 0, as said below
- lengths: int32 [16], P('dp'), may hold values from 32769 to 65536, as said below
- out_weight: bfloat16 [4096, 4096], P('tp', 'kv'), may hold values from -0.75 to 0.75
Outputs:
- mixed: bfloat16 [16, 4096], P('dp', 'kv')
Inputs may be any that keep to these rules, and one draw needn't show every extreme that they name: `gate_cache`: never rising along positions. `lengths`: in every draw some sequence has all 65536 positions cached.
All inputs are finite; a program needn't handle non-finite values.
Results may differ from a plain program's by a relative error of at most 0.012.
Values may be sent and summed in bfloat16 or wider, within the bound.
No kernel may reach another device: no remote copies, remote signals or barrier semaphores. Data moves between devices by JAX's collectives and lax.ppermute only.
A program may use at most 64 MiB of HBM per device.

v0:
```python
import jax
import jax.numpy as jnp
from jax import lax
from jax.sharding import Mesh
from jax.sharding import PartitionSpec as P

D = 4096
HEADS = 64
KV_HEADS = 8
HEAD = 64
KV = ("kv_0", "kv_1")


EPSILON = 1e-06
FLOOR = -1e30


def copy_for_each(array, axis):
    peers = lax.axis_size(axis)
    return lax.all_to_all(
        jnp.broadcast_to(array[None], (peers, *array.shape)), axis, 0, 0, tiled=True
    )


def taken_together(array, axis):
    everything = copy_for_each(array, axis)
    return jnp.sum(everything, axis=0)


def together(arrays, axis):
    ravelled, at, finished = (jnp.concatenate([a.reshape(-1) for a in arrays]), 0, [])
    so_far = taken_together(ravelled, axis)
    for a in arrays:
        finished.append(so_far[at : at + a.size].reshape(a.shape))
        at += a.size
    return tuple(finished)


def gathered_once(array, axis):
    leaves = jax.tree.leaves(array)
    turns = sorted(range(len(leaves)), key=lambda k: -leaves[k].size)
    width = (1, *leaves[turns[0]].shape)[-1]
    lines = [
        jnp.pad(leaves[k].reshape(-1), (0, -leaves[k].size % width)).reshape(-1, width)
        for k in turns
    ]
    both, at, found = (lax.all_gather(jnp.concatenate(lines), axis), 0, {})
    for k, line in zip(turns, lines):
        piece = both[:, at : at + len(line)].reshape(len(both), -1)
        found[k] = piece[:, : leaves[k].size].reshape(-1, *leaves[k].shape)
        at += len(line)
    numbers = iter(range(len(leaves)))
    return jax.tree.map(lambda _: found[next(numbers)], array)


def merged_by_axis(array, axes, combine):
    for axis in axes:
        pieces = gathered_once(array, axis)
        array = jax.tree.map(lambda part: part[0], pieces)
        for k in range(1, lax.axis_size(axis)):
            array = combine(array, jax.tree.map(lambda part: part[k], pieces))
    return array


def gathered_total(array, axis):
    return lax.all_gather(array, axis).astype(jnp.float32).sum(0)


def head_norm(values, gain):
    values = values.astype(jnp.float32)
    return values * lax.rsqrt(jnp.mean(values * values, axis=-1, keepdims=True) + EPSILON) * gain


def combine_parts(first, second):
    top = jnp.maximum(first[0], second[0])
    early = jnp.exp(first[0] - top)
    later = jnp.exp(second[0] - top)
    return (
        top,
        first[1] * early + second[1] * later,
        first[2] * early[..., None] + second[2] * later[..., None],
    )


def per_device(
    tokens,
    norm_gain,
    query_weight,
    key_weight,
    value_weight,
    gate_weight,
    gate_bias,
    query_gain,
    key_gain,
    key_cache,
    value_cache,
    gate_cache,
    lengths,
    out_weight,
):
    seqs, columns = tokens.shape
    kv_rank = lax.axis_index(KV)
    tp_rank = lax.axis_index("tp")
    key_width = key_weight.shape[1]
    groups = key_width // HEAD
    ratio = HEADS // KV_HEADS
    positions = key_cache.shape[1]
    tokens_f = tokens.astype(jnp.float32)
    squares = jnp.sum(tokens_f * tokens_f, axis=1)
    scaled = (tokens_f * norm_gain).astype(jnp.bfloat16)
    query_part = jnp.dot(scaled, query_weight, preferred_element_type=jnp.float32)
    key_part = jnp.dot(scaled, key_weight, preferred_element_type=jnp.float32)
    value_part = jnp.dot(scaled, value_weight, preferred_element_type=jnp.float32)
    gate_rows = lax.dynamic_slice(
        gate_weight, (kv_rank * columns, tp_rank * groups), (columns, groups)
    )
    gate_part = jnp.dot(scaled, gate_rows, preferred_element_type=jnp.float32)
    query_sum, key_sum, value_sum, gate_sum, square_sum = together(
        (query_part, key_part, value_part, gate_part, squares), KV
    )
    inverse = lax.rsqrt(square_sum / D + EPSILON)[:, None]
    query_raw = (query_sum * inverse).astype(jnp.bfloat16)
    key_raw = (key_sum * inverse).astype(jnp.bfloat16)
    value_raw = (value_sum * inverse).astype(jnp.bfloat16)
    local_bias = lax.dynamic_slice_in_dim(gate_bias, tp_rank * groups, groups)
    log_gate = jax.nn.log_sigmoid(gate_sum * inverse + local_bias)
    queries = head_norm(query_raw.reshape(seqs, groups, ratio, HEAD), query_gain).astype(
        jnp.bfloat16
    )
    key_new = head_norm(key_raw.reshape(seqs, groups, HEAD), key_gain).astype(jnp.bfloat16)
    value_new = value_raw.reshape(seqs, groups, HEAD).astype(jnp.float32)
    keys = key_cache.reshape(seqs, positions, groups, HEAD)
    values = value_cache.reshape(seqs, positions, groups, HEAD)
    scale = HEAD ** (-0.5)
    scores = (
        jnp.einsum("sgrd,spgd->sgrp", queries, keys, preferred_element_type=jnp.float32) * scale
    )
    scores = scores - gate_cache[:, :, None, :]
    offsets = jnp.arange(positions, dtype=jnp.int32)
    live = ((kv_rank * positions + offsets)[None, :] < lengths[:, None])[:, None, None, :]
    within = lengths - 1 - kv_rank * positions
    owner = ((within >= 0) & (within < positions))[:, None, None]
    picked = (offsets[None, :] == within[:, None])[:, None, :]
    last_gate = jnp.sum(jnp.where(picked, gate_cache, 0.0), axis=2)
    own_gate = last_gate + log_gate
    score_new = (
        jnp.einsum("sgrd,sgd->sgr", queries, key_new, preferred_element_type=jnp.float32) * scale
    )
    score_new = score_new - own_gate[:, :, None]
    maxima = jnp.max(jnp.where(live, scores, FLOOR), axis=3)
    maxima = jnp.where(owner, jnp.maximum(maxima, score_new), maxima)
    weights = jnp.where(live, jnp.exp(scores - maxima[..., None]), 0.0).astype(jnp.bfloat16)
    weight_new = (
        jnp.where(owner, jnp.exp(score_new - maxima), 0.0).astype(jnp.bfloat16).astype(jnp.float32)
    )
    totals = jnp.sum(weights.astype(jnp.float32), axis=3) + weight_new
    weighted = jnp.einsum("sgrp,spgd->sgrd", weights, values, preferred_element_type=jnp.float32)
    weighted = weighted + weight_new[..., None] * value_new[:, :, None, :]
    top, total, summed = merged_by_axis((maxima, totals, weighted), KV, combine_parts)
    attended = (summed / total[..., None]).astype(jnp.bfloat16).reshape(seqs, groups * ratio * HEAD)
    partial_value = jnp.dot(attended, out_weight, preferred_element_type=jnp.float32).astype(
        jnp.bfloat16
    )
    partial_value = lax.optimization_barrier(partial_value).astype(jnp.float32)
    return (
        gathered_total(partial_value.astype(jnp.bfloat16), "tp")
        .astype(jnp.float32)
        .astype(jnp.bfloat16)
    )


def solution(mesh):
    finer = Mesh(
        mesh.devices.reshape(mesh.shape["dp"], 8, 4, mesh.shape["tp"]), ("dp", "kv_0", "kv_1", "tp")
    )
    in_specs = (
        P("dp", KV),
        P(KV),
        P(KV, "tp"),
        P(KV, "tp"),
        P(KV, "tp"),
        P(),
        P(),
        P(),
        P(),
        P("dp", KV, "tp"),
        P("dp", KV, "tp"),
        P("dp", "tp", KV),
        P("dp"),
        P("tp", KV),
    )
    out_specs = P("dp", KV)
    return jax.shard_map(
        per_device, mesh=finer, in_specs=in_specs, out_specs=out_specs, check_vma=False
    )
```

profile of v0, /device:TPU:1, one launch (start us, length us, event | category | flops | bytes accessed | tf_op | source)
XLA Modules:
  0.0 109.6 jit_solution(6978354991441104752)
XLA Ops:
  0.0 0.9 fusion.40
  0.9 0.9 fusion.74
  1.8 0.1 reshape.759
  1.8 0.9 convolution_bitcast_fusion
  2.7 1.0 convolution_bitcast_fusion.2
  3.7 1.0 convolution_bitcast_fusion.1
  4.8 1.8 %broadcast_in_dim.51 = f32[32,1,10260]{2,1,0:T(1,128)} broadcast(f32[10260]{0:T(1024)S(1)} %concatenate.9), dimensions={2} | broadcast | bytes 1354320 | tf_op jit(solution)/shard_map/broadcast_in_dim | solution.py:21
  6.7 11.9 %all-to-all-start = ((f32[32,1,10260]{2,1,0:T(1,128)}), f32[32,1,10260]{2,1,0:T(1,128)S(1)}, u32[]{:S(2)}, u32[]{:S(2)}) async-start(f32[32,1,10260]{2,1,0:T(1,128)} %broadcast_in_dim.51), calls=%async_computation | async-start | bytes 2654208 | tf_op jit(solution)/shard_map/all_to_all | solution.py:20
  18.5 6.3 %copy.106 = bf16[4,2048,256]{1,2,0:T(8,128)(2,1)} copy(bf16[4,2048,256]{2,1,0:T(8,128)(2,1)} %param.23) | data formatting | bytes 8388608 | tf_op args[9]
  24.9 6.3 %copy.107 = bf16[4,2048,256]{1,2,0:T(8,128)(2,1)} copy(bf16[4,2048,256]{2,1,0:T(8,128)(2,1)} %param.24) | data formatting | bytes 8388608 | tf_op args[10]
  31.3 0.1 select_reduce_fusion.1
  31.5 19.3 %all-to-all-done = f32[32,1,10260]{2,1,0:T(1,128)S(1)} async-done(((f32[32,1,10260]{2,1,0:T(1,128)}), f32[32,1,10260]{2,1,0:T(1,128)S(1)}, u32[]{:S(2)}, u32[]{:S(2)}) %all-to-all-start) | async-done | bytes 1313312 | tf_op jit(solution)/shard_map/all_to_all | solution.py:20
  50.8 0.8 reduce_sum.67
  51.7 0.2 fusion.30
  52.0 0.2 fusion.1
  52.4 0.2 fusion.26
  52.6 3.0 %select_reduce_fusion = (f32[4,4,8]{2,1,0:T(4,128)S(1)}, f32[4,4,8,2048]{3,2,1,0:T(8,128)S(1)}) fusion(pred[4,2048]{1,0:T(4,128)(4,1)S(1)} %broadcast_compare_fusion, f32[4,4,2048]{2,1,0:T(4,128)S(1)} %copy-done.1, bf16[4,2048,4,64]{1,3,2,0:T(8,128)(2,1)} %bitcast.314, bf16[4,4,8,64]{3,2,1,0:T(8,128)(2,1)S(1)} %get-tuple-element.23, f32[64]{0:T(128)S(1)} %copy-done.4, ...), kind=kOutput, calls=%fused_computation.9 | convolution fusion | flops 34635648 | bytes 5399808 | tf_op jit(solution)/shard_map/sgrd,spgd->sgrp/dot_general | solution.py:136
  55.8 0.1 reshape.767
  55.9 0.4 convert_reduce_fusion
  56.3 3.4 %convolution_add_fusion = f32[4,4,8,64]{3,2,1,0:T(8,128)S(1)} fusion(bf16[4,2048,4,64]{1,3,2,0:T(8,128)(2,1)} %bitcast.315, f32[4,4,8,2048]{3,2,1,0:T(8,128)S(1)} %get-tuple-element.74, f32[4,4,8]{2,1,0:T(4,128)S(1)} %maximum_select_fusion, pred[4,2048]{1,0:T(4,128)(4,1)S(1)} %broadcast_compare_fusion, f32[4,4,64]{2,1,0:T(4,128)S(1)} %get-tuple-element.71, ...), kind=kOutput, calls=%fused_computation.2 | convolution fusion | flops 34357248 | bytes 5288960 | tf_op jit(solution)/shard_map/sgrp,spgd->sgrd/dot_general | solution.py:157
  59.8 0.1 reshape.768
  59.9 0.1 copy.110
  60.0 0.1 copy.109
  60.1 0.1 maximum_bitcast_fusion
  60.2 19.4 %all-gather.3 = f32[8,132,64]{1,2,0:T(8,128)S(1)} all-gather(f32[1,132,64]{1,2,0:T(8,128)S(1)} %maximum_bitcast_fusion), channel_id=2, replica_groups=mesh['dp'=4,'kv_0'=8,'kv_1'=4,'tp'=2] {'kv_0'}, dimensions={0}, use_global_device_ids=true | all-gather | bytes 304128 | tf_op jit(solution)/shard_map/all_gather | solution.py:47
  79.7 0.1 fusion.89
  80.0 0.1 squeeze.126
  81.7 0.1 bitcast_maximum_fusion
  81.8 0.1 copy.135
  81.9 0.1 copy.136
  82.2 11.0 %all-gather.4 = f32[4,132,64]{1,2,0:T(8,128)S(1)} all-gather(f32[1,132,64]{1,2,0:T(8,128)S(1)} %maximum_bitcast_fusion.1), channel_id=3, replica_groups=mesh['dp'=4,'kv_0'=8,'kv_1'=4,'tp'=2] {'kv_1'}, dimensions={0}, use_global_device_ids=true | all-gather | bytes 168960 | tf_op jit(solution)/shard_map/all_gather | solution.py:47
  93.2 0.1 fusion.91
  93.3 0.1 squeeze.167
  93.5 0.1 squeeze.166
  93.6 0.1 copy.146
  93.7 0.1 squeeze.165
  93.8 0.1 copy.145
  93.9 0.1 squeeze.164
  93.9 0.1 copy.138
  94.0 0.1 squeeze.157
  94.1 0.1 copy.139
  94.2 0.1 squeeze.158
  94.3 0.1 copy.141
  94.4 0.1 squeeze.160
  94.5 0.1 copy.143
  94.6 0.1 squeeze.162
  94.8 0.1 div.28
  94.9 0.1 mul.493
  95.1 0.1 mul.496
  95.3 0.1 mul.499
  95.5 0.1 mul.502
  95.7 0.1 mul.505
  95.8 0.1 mul.508
  95.9 0.1 copy.137
  96.0 0.1 squeeze.156
  96.1 0.1 copy.140
  96.2 0.1 squeeze.159
  96.3 0.1 copy.142
  96.4 0.1 squeeze.161
  96.5 0.1 copy.144
  96.6 0.1 squeeze.163
  96.7 0.2 convolution_convert_fusion
  96.9 12.1 %all-gather.5 = bf16[2,4,128]{2,1,0:T(4,128)(2,1)S(1)} all-gather(bf16[1,4,128]{2,1,0:T(4,128)(2,1)S(1)} %bitcast.337), channel_id=4, replica_groups=mesh['dp'=4,'kv_0'=8,'kv_1'=4,'tp'=2] {'tp'}, dimensions={0}, use_global_device_ids=true | all-gather | bytes 3072 | tf_op jit(solution)/shard_map/all_gather | solution.py:66
  109.0 0.6 reduce_sum.72
  (78 shorter events, 3.8 us)
Async XLA Ops:
  0.0 1.8 %copy-start = (bf16[128,2048]{1,0:T(8,128)(2,1)S(1)}, bf16[128,2048]{1,0:T(8,128)(2,1)}, u32[]{:S(2)}) copy-start(bf16[128,2048]{1,0:T(8,128)(2,1)} %param.16) | copy-start | bytes 1572868
  6.7 44.1 %all-to-all-start = ((f32[32,1,10260]{2,1,0:T(1,128)}), f32[32,1,10260]{2,1,0:T(1,128)S(1)}, u32[]{:S(2)}, u32[]{:S(2)}) async-start(f32[32,1,10260]{2,1,0:T(1,128)} %broadcast_in_dim.51), calls=%async_computation | async-start | bytes 2654208 | tf_op jit(solution)/shard_map/all_to_all | solution.py:20
  18.5 6.3 %copy-start.6 = (f32[8]{0:T(128)S(1)}, f32[8]{0:T(128)}, u32[]{:S(2)}) copy-start(f32[8]{0:T(128)} %param.20) | copy-start | bytes 100
  24.9 6.3 %copy-start.3 = (s32[4]{0:T(128)S(1)}, s32[4]{0:T(128)}, u32[]{:S(2)}) copy-start(s32[4]{0:T(128)} %param.26) | copy-start | bytes 52
  24.9 6.4 %copy-start.1 = (f32[4,4,2048]{2,1,0:T(4,128)S(1)}, f32[4,4,2048]{2,1,0:T(4,128)}, u32[]{:S(2)}) copy-start(f32[4,4,2048]{2,1,0:T(4,128)} %param.25) | copy-start | bytes 393220
  24.9 27.4 %copy-start.5 = (f32[64]{0:T(128)S(1)}, f32[64]{0:T(128)}, u32[]{:S(2)}) copy-start(f32[64]{0:T(128)} %param.22) | copy-start | bytes 772
  24.9 27.5 %copy-start.4 = (f32[64]{0:T(128)S(1)}, f32[64]{0:T(128)}, u32[]{:S(2)}) copy-start(f32[64]{0:T(128)} %param.21) | copy-start | bytes 772
  59.8 36.9 %copy-start.2 = (bf16[2048,128]{1,0:T(8,128)(2,1)S(1)}, bf16[2048,128]{1,0:T(8,128)(2,1)}, u32[]{:S(2)}) copy-start(bf16[2048,128]{1,0:T(8,128)(2,1)} %param.27) | copy-start | bytes 1572868
where the time goes:
time: 110 us
  blocking collectives  42.5 us (39%)
  local copies, waits for them, and re-layouts  21.1 us (19%)
  waiting for transfers between devices  19.3 us (18%)
  starting transfers between devices  11.9 us (11%)
  matrix products  10.6 us (10%)
  other arithmetic  4 us (4%)
    all_gather x2, blocking collectives, gathered_once(): both, at, found = (lax.all_gather(jnp.concatenate(lines), axis), 0, {})  30.4 us
    all_to_all x1, waiting for transfers between devices, copy_for_each(): lax.all_to_all(jnp.broadcast_to(array[None], (peers, *array.shape)), axis...  19.3 us
    unnamed x19, local copies, waits for them, and re-layouts  12.6 us
    all_gather x1, blocking collectives, gathered_total(): return lax.all_gather(array, axis).astype(jnp.float32).sum(0)  12.1 us
    all_to_all x1, starting transfers between devices, copy_for_each(): lax.all_to_all(jnp.broadcast_to(array[None], (peers, *array.shape)), axis...  11.9 us
    dot_general x1, matrix products, per_device(): jnp.einsum('sgrp,spgd->sgrd', weights, values, preferred_element_type=jnp...  3.43 us
    dot_general x1, matrix products, per_device(): jnp.einsum('sgrd,spgd->sgrp', queries, keys, preferred_element_type=jnp.f...  3 us
  transfers between devices with their start and end apart: 1, of which 1 were waited for; matrix products, arithmetic and copies ran while one was open for 12% of the time, Pallas kernels for 0%

commit v1 on v0

v1 whole, which is shorter than its diff:
```python
import functools

import jax
import jax.numpy as jnp
from jax import lax
from jax.experimental import pallas as pl
from jax.experimental.pallas import tpu as pltpu
from jax.sharding import Mesh
from jax.sharding import PartitionSpec as P

D = 4096
HEADS = 64
KV_HEADS = 8
HEAD = 64
KV = ("kv_0", "kv_1")

EPSILON = 1e-06
FLOOR = -1e30
VMEM = pltpu.VMEM
F32 = jnp.float32
BF16 = jnp.bfloat16


def lanes_of(shape):
    return lax.broadcasted_iota(jnp.int32, shape, 1)


def halves_stacked(part):
    half = part.shape[1] // 2
    return jnp.concatenate([part[:, :half], part[:, half:]], axis=0)


def project_kernel(tokens_ref, gain_ref, query_ref, key_ref, value_ref, gate_ref, out_ref):
    tokens = tokens_ref[...].astype(F32)
    squares = jnp.sum(tokens * tokens, axis=1, keepdims=True)
    scaled = (tokens * gain_ref[...]).astype(BF16)
    query = jnp.dot(scaled, query_ref[...], preferred_element_type=F32)
    key = jnp.dot(scaled, key_ref[...], preferred_element_type=F32)
    value = jnp.dot(scaled, value_ref[...], preferred_element_type=F32)
    gate = jnp.dot(scaled, gate_ref[...], preferred_element_type=F32)
    extra = gate + jnp.where(lanes_of(gate.shape) == 4, squares, 0.0)
    extra = jnp.concatenate([extra, jnp.zeros_like(extra)], axis=0)
    whole = jnp.concatenate(
        [halves_stacked(query), halves_stacked(key), halves_stacked(value), extra], axis=1
    ).astype(BF16)
    for copy in range(out_ref.shape[0]):
        out_ref[copy] = whole


def split_heads_sum(squares):
    row = lax.broadcasted_iota(jnp.int32, (128, 128), 0) // HEAD
    column = lanes_of((128, 128)) // HEAD
    ones = jnp.where(row == column, 1.0, 0.0).astype(BF16)
    high = squares.astype(BF16)
    low = (squares - high.astype(F32)).astype(BF16)
    return jnp.dot(high, ones, preferred_element_type=F32) + jnp.dot(
        low, ones, preferred_element_type=F32
    )


def attend_kernel(
    rest_ref, sums_ref, small_ref, gate_ref, key_ref, value_ref, out_ref, query_ref
):
    seqs, positions = gate_ref.shape[0], gate_ref.shape[2]
    total = sums_ref[0].astype(F32)
    for piece in range(1, sums_ref.shape[0]):
        total = total + sums_ref[piece].astype(F32)
    extra = total[:, 1280:]
    inverse = lax.rsqrt(extra[0:seqs, 4:5] / D + EPSILON)
    inverse = jnp.concatenate([inverse, inverse], axis=0)
    raw = (total[:, :1280] * inverse).astype(BF16).astype(F32)
    tiles = [raw[:, 128 * k : 128 * (k + 1)] for k in range(10)]
    values_new = tiles[9]
    stacked = jnp.concatenate(tiles[:9], axis=0)
    mean = split_heads_sum(stacked * stacked) * (1.0 / HEAD)
    normed = stacked * lax.rsqrt(mean + EPSILON)
    query_ref[...] = (normed[:64] * small_ref[0:1, :]).astype(BF16).astype(F32)
    keys_new = (normed[64:] * small_ref[1:2, :]).astype(BF16).astype(F32)
    logit = extra * inverse + small_ref[2:3, :]
    log_gate = jnp.minimum(logit, 0.0) - jnp.log1p(jnp.exp(-jnp.abs(logit)))

    lane = lanes_of((8, 128))
    row = lax.broadcasted_iota(jnp.int32, (8, 128), 0)
    left, early = lane < HEAD, row < 4
    place = lanes_of((8, positions))
    early_wide = lax.broadcasted_iota(jnp.int32, (8, positions), 0) < 4
    maxima = jnp.zeros((8, 128), F32)
    sums = jnp.zeros((8, 128), F32)
    for s in range(seqs):
        rest = rest_ref[s]
        owner = jnp.logical_and(rest >= 1, rest <= positions)
        live = place < rest
        chosen = place == rest - 1
        parts, gates, last, fresh = [], [], [], []
        for a in range(2):
            heads = query_ref[pl.ds(a * seqs + s, 8, stride=8), :]
            turned = pltpu.roll(heads, HEAD, 1)
            even = jnp.where(left == early, jnp.where(early, heads, turned), 0.0)
            odd = jnp.where(left == early, jnp.where(early, turned, heads), 0.0)
            parts.append(jnp.concatenate([even, odd], axis=0) * HEAD ** (-0.5))
            gate = jnp.where(
                early_wide, gate_ref[s, 2 * a : 2 * a + 1, :], gate_ref[s, 2 * a + 1 : 2 * a + 2, :]
            )
            gates.append(gate)
            own = jnp.sum(jnp.where(chosen, gate, 0.0), axis=1, keepdims=True)
            wanted = jnp.where(early, 2 * a, 2 * a + 1)
            own = own + jnp.sum(
                jnp.where(lane == wanted, log_gate[s : s + 1, :], 0.0), axis=1, keepdims=True
            )
            new = jnp.sum(
                parts[a] * keys_new[a * seqs + s : a * seqs + s + 1, :], axis=1, keepdims=True
            )
            fresh.append(new - jnp.concatenate([own, own], axis=0))
        zeros = jnp.zeros((16, 128), F32)
        query = jnp.concatenate(
            [
                jnp.concatenate([parts[0], zeros], axis=1),
                jnp.concatenate([zeros, parts[1]], axis=1),
            ],
            axis=0,
        ).astype(BF16)
        scores = lax.dot_general(
            query, key_ref[s], (((1,), (1,)), ((), ())), preferred_element_type=F32
        )
        gate = jnp.concatenate([gates[0], gates[0], gates[1], gates[1]], axis=0)
        live = jnp.concatenate([live] * 4, axis=0)
        scores = jnp.where(live, scores - gate, FLOOR)
        top = jnp.max(scores, axis=1, keepdims=True)
        score_new = jnp.concatenate(fresh, axis=0)
        top = jnp.where(owner, jnp.maximum(top, score_new), top)
        weights = jnp.where(live, jnp.exp(scores - top), 0.0).astype(BF16)
        weight_new = jnp.where(owner, jnp.exp(score_new - top), 0.0).astype(BF16).astype(F32)
        count = jnp.sum(weights.astype(F32), axis=1, keepdims=True) + weight_new
        summed = jnp.dot(weights, value_ref[s], preferred_element_type=F32)
        for a in range(2):
            rows = slice(16 * a, 16 * a + 16)
            mine = summed[rows, 128 * a : 128 * a + 128]
            mine = mine + weight_new[rows] * values_new[a * seqs + s : a * seqs + s + 1, :]
            even, odd = mine[:8], mine[8:]
            dense = jnp.where(
                left,
                jnp.where(early, even, pltpu.roll(even, HEAD, 1)),
                jnp.where(early, pltpu.roll(odd, HEAD, 1), odd),
            ).astype(BF16)
            at = 8 * (2 * s + a)
            for copy in range(out_ref.shape[0]):
                out_ref[copy, at : at + 8, :] = dense
            for p in range(2):
                here = lane == 4 * s + 2 * a + p
                own_rows = slice(16 * a + 8 * p, 16 * a + 8 * p + 8)
                maxima = jnp.where(here, top[own_rows], maxima)
                sums = jnp.where(here, count[own_rows], sums)
    packed = pack_statistics(maxima, sums)
    for copy in range(out_ref.shape[0]):
        out_ref[copy, 64:72, :] = packed


def pack_statistics(maxima, sums):
    first = maxima.astype(BF16).astype(F32)
    second = (maxima - first).astype(BF16).astype(F32)
    third = (maxima - first - second).astype(BF16).astype(F32)
    high = sums.astype(BF16).astype(F32)
    low = (sums - high).astype(BF16).astype(F32)
    packed = first + pltpu.roll(second, 16, 1) + pltpu.roll(third, 32, 1)
    packed = packed + pltpu.roll(high, 48, 1) + pltpu.roll(low, 64, 1)
    return packed.astype(BF16)


def unpack_statistics(packed):
    packed = packed.astype(F32)
    valid = lanes_of((8, 128)) < 16
    maxima = packed + pltpu.roll(packed, 112, 1) + pltpu.roll(packed, 96, 1)
    sums = pltpu.roll(packed, 80, 1) + pltpu.roll(packed, 64, 1)
    return jnp.where(valid, maxima, 0.0), jnp.where(valid, sums, 0.0)


def spread(tile, k):
    left = lanes_of((8, 128)) < HEAD
    return jnp.where(left, tile[:, 2 * k : 2 * k + 1], tile[:, 2 * k + 1 : 2 * k + 2])


def merged(in_ref):
    pieces = in_ref.shape[0]
    found = [unpack_statistics(in_ref[i, 64:72, :]) for i in range(pieces)]
    top = functools.reduce(jnp.maximum, [maxima for maxima, _ in found])
    factors = [jnp.exp(maxima - top) for maxima, _ in found]
    total = sum(factor * sums for factor, (_, sums) in zip(factors, found))
    values = []
    for k in range(8):
        values.append(
            sum(
                in_ref[i, 8 * k : 8 * k + 8, :].astype(F32) * spread(factors[i], k)
                for i in range(pieces)
            )
        )
    return top, total, values


def merge_kernel(in_ref, out_ref):
    top, total, values = merged(in_ref)
    packed = pack_statistics(top, total)
    dense = jnp.concatenate(values, axis=0).astype(BF16)
    for copy in range(out_ref.shape[0]):
        out_ref[copy, :64, :] = dense
        out_ref[copy, 64:72, :] = packed


def finish_kernel(in_ref, weight_ref, out_ref, attended_ref):
    top, total, values = merged(in_ref)
    for k in range(8):
        attended_ref[8 * k : 8 * k + 8, :] = values[k] / spread(total, k)
    attended = jnp.concatenate(
        [attended_ref[pl.ds(k, 4, stride=16), :] for k in range(16)], axis=1
    ).astype(BF16)
    out_ref[...] = jnp.dot(attended, weight_ref[...], preferred_element_type=F32).astype(BF16)


def limit(mebibytes):
    return pltpu.CompilerParams(vmem_limit_bytes=mebibytes << 20)


def in_vmem(count):
    return [pl.BlockSpec(memory_space=VMEM)] * count


def exchanged(array, axis):
    return lax.all_to_all(array, axis, 0, 0, tiled=True)


def per_device(
    tokens,
    norm_gain,
    query_weight,
    key_weight,
    value_weight,
    gate_weight,
    gate_bias,
    query_gain,
    key_gain,
    key_cache,
    value_cache,
    gate_cache,
    lengths,
    out_weight,
):
    seqs, columns = tokens.shape
    kv_rank = lax.axis_index(KV)
    tp_rank = lax.axis_index("tp")
    groups = key_weight.shape[1] // HEAD
    positions = key_cache.shape[1]
    outer, inner = lax.axis_size("kv_0"), lax.axis_size("kv_1")
    gate_rows = lax.dynamic_slice(
        gate_weight, (kv_rank * columns, tp_rank * groups), (columns, groups)
    )
    gate_rows = jnp.pad(gate_rows, ((0, 0), (0, 128 - groups)))
    local_bias = lax.dynamic_slice_in_dim(gate_bias, tp_rank * groups, groups)
    small = jnp.stack(
        [jnp.tile(query_gain, 2), jnp.tile(key_gain, 2), jnp.pad(local_bias, (0, 128 - groups))]
    )
    rest = lengths - kv_rank * positions

    sums = pl.pallas_call(
        project_kernel,
        out_shape=jax.ShapeDtypeStruct((inner, 8, 1408), BF16),
        in_specs=in_vmem(6),
        out_specs=in_vmem(1)[0],
        compiler_params=limit(4),
        name="project",
    )(tokens, norm_gain[None], query_weight, key_weight, value_weight, gate_rows)
    sums = exchanged(sums, "kv_1").astype(F32).sum(0).astype(BF16)
    sums = exchanged(jnp.broadcast_to(sums[None], (outer, 8, 1408)), "kv_0")
    parts = pl.pallas_call(
        attend_kernel,
        out_shape=jax.ShapeDtypeStruct((inner, 72, 128), BF16),
        in_specs=[pl.BlockSpec(memory_space=pltpu.SMEM)] + in_vmem(5),
        out_specs=in_vmem(1)[0],
        scratch_shapes=[VMEM((64, 128), F32)],
        compiler_params=limit(24),
        name="attend",
    )(rest, sums, small, gate_cache, key_cache, value_cache)
    parts = pl.pallas_call(
        merge_kernel,
        out_shape=jax.ShapeDtypeStruct((outer, 72, 128), BF16),
        in_specs=in_vmem(1),
        out_specs=in_vmem(1)[0],
        compiler_params=limit(4),
        name="merge",
    )(exchanged(parts, "kv_1"))
    mixed = pl.pallas_call(
        finish_kernel,
        out_shape=jax.ShapeDtypeStruct((seqs, out_weight.shape[1]), BF16),
        in_specs=in_vmem(2),
        out_specs=in_vmem(1)[0],
        scratch_shapes=[VMEM((64, 128), F32)],
        compiler_params=limit(4),
        name="finish",
    )(exchanged(parts, "kv_0"), out_weight)
    other = lax.ppermute(mixed, "tp", [(0, 1), (1, 0)])
    return (mixed.astype(F32) + other.astype(F32)).astype(BF16)


def solution(mesh):
    finer = Mesh(
        mesh.devices.reshape(mesh.shape["dp"], 8, 4, mesh.shape["tp"]), ("dp", "kv_0", "kv_1", "tp")
    )
    in_specs = (
        P("dp", KV),
        P(KV),
        P(KV, "tp"),
        P(KV, "tp"),
        P(KV, "tp"),
        P(),
        P(),
        P(),
        P(),
        P("dp", KV, "tp"),
        P("dp", KV, "tp"),
        P("dp", "tp", KV),
        P("dp"),
        P("tp", KV),
    )
    out_specs = P("dp", KV)
    return jax.shard_map(
        per_device, mesh=finer, in_specs=in_specs, out_specs=out_specs, check_vma=False
    )
```

time: 110 us -> 68.2 us (0.62)
  blocking collectives: 42.5 us -> 17.4 us
  matrix products: 10.6 us -> 0 us
  waiting for transfers between devices: 19.3 us -> 11.1 us
  local copies, waits for them, and re-layouts: 21.1 us -> 13.1 us
  starting transfers between devices: 11.9 us -> 18.8 us
  Pallas kernels: 0 us -> 5.92 us
  other arithmetic: 4 us -> 1.25 us
    all_gather x3 -> x0, blocking collectives: 42.5 us -> none  [the longest x2 30.4 us: gathered_once(): both, at, found = (lax.all_gather(jnp.concatenate(lines), axis), 0, {})]
    all_to_all x0 -> x2, blocking collectives: none -> 17.4 us  [exchanged(): return lax.all_to_all(array, axis, 0, 0, tiled=True)]
    dot_general x8 -> x0, matrix products: 10.6 us -> none  [the longest x1 3.43 us: per_device(): jnp.einsum('sgrp,spgd->sgrd', weights, values, preferred_element_type=jnp...]
    all_to_all x1 -> x2, waiting for transfers between devices: 19.3 us -> 10.3 us  [exchanged(): return lax.all_to_all(array, axis, 0, 0, tiled=True)]
    pallas_call x0 -> x4, Pallas kernels: none -> 5.92 us  [the longest x1 4.26 us: per_device(): pl.pallas_call(attend_kernel, out_shape=jax.ShapeDtypeStruct((inner, 72,...]
    ppermute x0 -> x1, starting transfers between devices: none -> 5.76 us  [per_device(): other = lax.ppermute(mixed, 'tp', [(0, 1), (1, 0)])]
    unnamed x19, local copies, waits for them, and re-layouts: 12.6 us -> 9.47 us
    reduce_sum x7 -> x1, other arithmetic: 3.02 us -> 0.02 us  [per_device(): sums = exchanged(sums, 'kv_1').astype(F32).sum(0).astype(BF16)]
  transfers between devices with their start and end apart: 1 -> 3, of which waited for: 1 -> 3; matrix products, arithmetic and copies ran while one was open for 12% -> 4% of each run, Pallas kernels for 0% -> 0%
where the time goes in v1:
time: 68.2 us; the launch traced here: 67.6 us
  starting transfers between devices  18.8 us (28%)
  blocking collectives  17.4 us (26%)
  local copies, waits for them, and re-layouts  13.1 us (19%)
  waiting for transfers between devices  11.1 us (16%)
  Pallas kernels  5.92 us (9%)
  other arithmetic  1.25 us (2%)
    all_to_all x2, blocking collectives, exchanged(): return lax.all_to_all(array, axis, 0, 0, tiled=True)  17.4 us
    all_to_all x2, starting transfers between devices, exchanged(): return lax.all_to_all(array, axis, 0, 0, tiled=True)  13 us
    all_to_all x2, waiting for transfers between devices, exchanged(): return lax.all_to_all(array, axis, 0, 0, tiled=True)  10.3 us
    unnamed x19, local copies, waits for them, and re-layouts  9.47 us
    ppermute x1, starting transfers between devices, per_device(): other = lax.ppermute(mixed, 'tp', [(0, 1), (1, 0)])  5.76 us
    pallas_call x1, Pallas kernels, per_device(): pl.pallas_call(attend_kernel, out_shape=jax.ShapeDtypeStruct((inner, 72,...  4.26 us
  transfers between devices with their start and end apart: 3, of which 3 were waited for; matrix products, arithmetic and copies ran while one was open for 4% of the time, Pallas kernels for 0%

profile of v1, /device:TPU:1, one launch (start us, length us, event | category | flops | bytes accessed | tf_op | source)
XLA Modules:
  0.0 67.6 jit_solution(4452284056560302874)
XLA Ops:
  0.0 0.8 %dynamic_slice.6 = bf16[128,4]{0,1:T(4,128)(2,1)S(1)} dynamic-slice(bf16[4096,8]{0,1:T(8,128)(2,1)} %param.19, s32[]{:T(128)S(6)} %select_n.7, s32[]{:T(128)S(6)} %select_n.8), dynamic_slice_sizes={128,4} | dynamic-slice | bytes 2052 | tf_op jit(solution)/shard_map/dynamic_slice | solution.py:252
  0.8 0.1 copy.16
  0.9 0.0 copy-start.2
  0.9 1.0 %copy-done.2 = bf16[128,2048]{1,0:T(8,128)(2,1)S(1)} copy-done((bf16[128,2048]{1,0:T(8,128)(2,1)S(1)}, bf16[128,2048]{1,0:T(8,128)(2,1)}, u32[]{:S(2)}) %copy-start.2) | copy-done | bytes 524312
  2.0 0.0 copy-start.5
  2.0 0.8 %copy-done.5 = bf16[128,256]{1,0:T(8,128)(2,1)S(1)} copy-done((bf16[128,256]{1,0:T(8,128)(2,1)S(1)}, bf16[128,256]{1,0:T(8,128)(2,1)}, u32[]{:S(2)}) %copy-start.5) | copy-done | bytes 65560
  2.8 0.0 copy-start.6
  2.8 0.8 %copy-done.6 = bf16[128,256]{1,0:T(8,128)(2,1)S(1)} copy-done((bf16[128,256]{1,0:T(8,128)(2,1)S(1)}, bf16[128,256]{1,0:T(8,128)(2,1)}, u32[]{:S(2)}) %copy-start.6) | copy-done | bytes 65560
  3.6 0.0 copy-start.7
  3.6 0.7 %copy-done.7 = bf16[4,128]{1,0:T(4,128)(2,1)S(1)} copy-done((bf16[4,128]{1,0:T(4,128)(2,1)S(1)}, bf16[4,128]{1,0:T(4,128)(2,1)}, u32[]{:S(2)}) %copy-start.7) | copy-done | bytes 1048
  4.3 0.0 copy-start.8
  4.3 0.7 copy-done.8
  5.0 0.9 %project.1 = bf16[4,8,1408]{2,1,0:T(8,128)(2,1)} custom-call(bf16[4,128]{1,0:T(4,128)(2,1)S(1)} %copy-done.7, f32[1,128]{1,0:T(1,128)S(1)} %bitcast.3, bf16[128,2048]{1,0:T(8,128)(2,1)S(1)} %copy-done.2, bf16[128,256]{1,0:T(8,128)(2,1)S(1)} %copy-done.5, bf16[128,256]{1,0:T(8,128)(2,1)S(1)} %copy-done.6, bf16[128,128]{1,0:T(8,128)(2,1)S(1)} %pad.8.gate_ref), custom_call_target="tpu_custom_call" | custom-call | tf_op jit(solution)/shard_map/project/pallas_call | solution.py:262
  5.8 4.8 %all-to-all-start = ((bf16[4,8,1408]{2,1,0:T(8,128)(2,1)}), bf16[4,8,1408]{2,1,0:T(8,128)(2,1)S(1)}, u32[]{:S(2)}, u32[]{:S(2)}) async-start(bf16[4,8,1408]{2,1,0:T(8,128)(2,1)} %project.1), calls=%async_computation | async-start | bytes 180224 | tf_op jit(solution)/shard_map/all_to_all | solution.py:227
  10.7 0.7 %dynamic_slice.7 = f32[4]{0:T(128)S(1)} dynamic-slice(f32[8]{0:T(128)} %param.20, s32[]{:T(128)S(6)} %select_n.8), dynamic_slice_sizes={4} | dynamic-slice | bytes 36 | tf_op jit(solution)/shard_map/dynamic_slice | solution.py:256
  11.4 0.7 tile.4
  12.0 0.1 stack_tile.6
  12.1 0.7 tile.5
  12.8 0.1 stack_tile.7
  12.9 2.4 %all-to-all-done = bf16[4,8,1408]{2,1,0:T(8,128)(2,1)S(1)} async-done(((bf16[4,8,1408]{2,1,0:T(8,128)(2,1)}), bf16[4,8,1408]{2,1,0:T(8,128)(2,1)S(1)}, u32[]{:S(2)}, u32[]{:S(2)}) %all-to-all-start) | async-done | bytes 90144 | tf_op jit(solution)/shard_map/all_to_all | solution.py:227
  15.3 0.7 %broadcast_in_dim.10 = bf16[8,8,1408]{2,1,0:T(8,128)(2,1)} broadcast(bf16[8,1408]{1,0:T(8,128)(2,1)S(1)} %reduce_sum.12), dimensions={1,2} | broadcast | bytes 202752 | tf_op jit(solution)/shard_map/broadcast_in_dim | solution.py:271
  16.0 8.2 %all-to-all-start.1 = ((bf16[8,8,1408]{2,1,0:T(8,128)(2,1)}), bf16[8,8,1408]{2,1,0:T(8,128)(2,1)S(1)}, u32[]{:S(2)}, u32[]{:S(2)}) async-start(bf16[8,8,1408]{2,1,0:T(8,128)(2,1)} %broadcast_in_dim.10), calls=%async_computation.1 | async-start | bytes 360448 | tf_op jit(solution)/shard_map/all_to_all | solution.py:227
  24.2 0.7 broadcast_subtract_fusion.rest_ref
  24.8 7.9 %all-to-all-done.1.sums_ref = bf16[8,8,1408]{2,1,0:T(8,128)(2,1)S(1)} async-done(((bf16[8,8,1408]{2,1,0:T(8,128)(2,1)}), bf16[8,8,1408]{2,1,0:T(8,128)(2,1)S(1)}, u32[]{:S(2)}, u32[]{:S(2)}) %all-to-all-start.1) | async-done | bytes 180256 | tf_op jit(solution)/shard_map/all_to_all | solution.py:227
  32.7 0.0 copy-start
  32.7 2.2 %copy-done = bf16[4,2048,256]{2,1,0:T(8,128)(2,1)S(1)} copy-done((bf16[4,2048,256]{2,1,0:T(8,128)(2,1)S(1)}, bf16[4,2048,256]{2,1,0:T(8,128)(2,1)}, u32[]{:S(2)}) %copy-start) | copy-done | bytes 4194328
  34.9 0.0 copy-start.1
  34.9 2.2 %copy-done.1 = bf16[4,2048,256]{2,1,0:T(8,128)(2,1)S(1)} copy-done((bf16[4,2048,256]{2,1,0:T(8,128)(2,1)S(1)}, bf16[4,2048,256]{2,1,0:T(8,128)(2,1)}, u32[]{:S(2)}) %copy-start.1) | copy-done | bytes 4194328
  37.1 0.0 copy-start.4
  37.1 0.9 %copy-done.4 = f32[4,4,2048]{2,1,0:T(4,128)S(1)} copy-done((f32[4,4,2048]{2,1,0:T(4,128)S(1)}, f32[4,4,2048]{2,1,0:T(4,128)}, u32[]{:S(2)}) %copy-start.4) | copy-done | bytes 131096
  38.0 0.0 copy-start.3
  38.0 4.3 %attend.1 = bf16[4,72,128]{2,1,0:T(8,128)(2,1)S(1)} custom-call(s32[4]{0:T(128)S(1)} %broadcast_subtract_fusion.rest_ref, bf16[8,8,1408]{2,1,0:T(8,128)(2,1)S(1)} %all-to-all-done.1.sums_ref, f32[3,128]{1,0:T(4,128)S(1)} %pad_maximum_fusion.small_ref, f32[4,4,2048]{2,1,0:T(4,128)S(1)} %copy-done.4, bf16[4,2048,256]{2,1,0:T(8,128)(2,1)S(1)} %copy-done, ...), custom_call_target="tpu_custom_call" | custom-call | tf_op jit(solution)/shard_map/attend/pallas_call | solution.py:272
  42.3 6.9 %all_to_all.20.in_ref = bf16[4,72,128]{2,1,0:T(8,128)(2,1)S(1)} all-to-all(bf16[4,72,128]{2,1,0:T(8,128)(2,1)S(1)} %attend.1), channel_id=1, replica_groups=mesh['dp'=4,'kv_0'=8,'kv_1'=4,'tp'=2] {'kv_1'}, dimensions={0} | all-to-all | bytes 147456 | tf_op jit(solution)/shard_map/all_to_all | solution.py:227
  49.1 0.3 merge.1
  49.4 10.5 %all_to_all.21.in_ref = bf16[8,72,128]{2,1,0:T(8,128)(2,1)S(1)} all-to-all(bf16[8,72,128]{2,1,0:T(8,128)(2,1)S(1)} %merge.1), channel_id=1, replica_groups=mesh['dp'=4,'kv_0'=8,'kv_1'=4,'tp'=2] {'kv_0'}, dimensions={0} | all-to-all | bytes 294912 | tf_op jit(solution)/shard_map/all_to_all | solution.py:227
  59.9 0.0 copy-done.3
  59.9 0.5 finish.1
  60.4 5.8 %collective-permute-start = (bf16[4,128]{1,0:T(4,128)(2,1)S(1)}, bf16[4,128]{1,0:T(4,128)(2,1)S(1)}, u32[]{:S(2)}, u32[]{:S(2)}) collective-permute-start(bf16[4,128]{1,0:T(4,128)(2,1)S(1)} %finish.1), channel_id=1, source_target_pairs={{0,1},{1,0},{2,3},{3,2},{4,5},{5,4},{6,7},{7,6},{8,9},{9,8},{10,11... | collective-permute-start | bytes 3080 | tf_op jit(solution)/shard_map/ppermute | solution.py:298
  66.2 0.8 %collective-permute-done = bf16[4,128]{1,0:T(4,128)(2,1)S(1)} collective-permute-done((bf16[4,128]{1,0:T(4,128)(2,1)S(1)}, bf16[4,128]{1,0:T(4,128)(2,1)S(1)}, u32[]{:S(2)}, u32[]{:S(2)}) %collective-permute-start) | collective-permute-done | bytes 1056 | tf_op jit(solution)/shard_map/ppermute | solution.py:298
  67.0 0.6 add_convert_fusion
  (4 shorter events, 0.0 us)
Async XLA Ops:
  0.9 1.0 %copy-start.2 = (bf16[128,2048]{1,0:T(8,128)(2,1)S(1)}, bf16[128,2048]{1,0:T(8,128)(2,1)}, u32[]{:S(2)}) copy-start(bf16[128,2048]{1,0:T(8,128)(2,1)} %query_ref.1) | copy-start | bytes 1572868
  2.0 0.8 %copy-start.5 = (bf16[128,256]{1,0:T(8,128)(2,1)S(1)}, bf16[128,256]{1,0:T(8,128)(2,1)}, u32[]{:S(2)}) copy-start(bf16[128,256]{1,0:T(8,128)(2,1)} %key_ref.2) | copy-start | bytes 196612
  2.8 0.8 %copy-start.6 = (bf16[128,256]{1,0:T(8,128)(2,1)S(1)}, bf16[128,256]{1,0:T(8,128)(2,1)}, u32[]{:S(2)}) copy-start(bf16[128,256]{1,0:T(8,128)(2,1)} %value_ref.2) | copy-start | bytes 196612
  3.6 0.7 %copy-start.7 = (bf16[4,128]{1,0:T(4,128)(2,1)S(1)}, bf16[4,128]{1,0:T(4,128)(2,1)}, u32[]{:S(2)}) copy-start(bf16[4,128]{1,0:T(4,128)(2,1)} %tokens_ref.1) | copy-start | bytes 3076
  4.3 0.7 copy-start.8
  5.8 9.4 %all-to-all-start = ((bf16[4,8,1408]{2,1,0:T(8,128)(2,1)}), bf16[4,8,1408]{2,1,0:T(8,128)(2,1)S(1)}, u32[]{:S(2)}, u32[]{:S(2)}) async-start(bf16[4,8,1408]{2,1,0:T(8,128)(2,1)} %project.1), calls=%async_computation | async-start | bytes 180224 | tf_op jit(solution)/shard_map/all_to_all | solution.py:227
  16.0 16.7 %all-to-all-start.1 = ((bf16[8,8,1408]{2,1,0:T(8,128)(2,1)}), bf16[8,8,1408]{2,1,0:T(8,128)(2,1)S(1)}, u32[]{:S(2)}, u32[]{:S(2)}) async-start(bf16[8,8,1408]{2,1,0:T(8,128)(2,1)} %broadcast_in_dim.10), calls=%async_computation.1 | async-start | bytes 360448 | tf_op jit(solution)/shard_map/all_to_all | solution.py:227
  32.7 2.2 %copy-start = (bf16[4,2048,256]{2,1,0:T(8,128)(2,1)S(1)}, bf16[4,2048,256]{2,1,0:T(8,128)(2,1)}, u32[]{:S(2)}) copy-start(bf16[4,2048,256]{2,1,0:T(8,128)(2,1)} %key_ref.3) | copy-start | bytes 12582916
  34.9 2.2 %copy-start.1 = (bf16[4,2048,256]{2,1,0:T(8,128)(2,1)S(1)}, bf16[4,2048,256]{2,1,0:T(8,128)(2,1)}, u32[]{:S(2)}) copy-start(bf16[4,2048,256]{2,1,0:T(8,128)(2,1)} %value_ref.3) | copy-start | bytes 12582916
  37.1 0.9 %copy-start.4 = (f32[4,4,2048]{2,1,0:T(4,128)S(1)}, f32[4,4,2048]{2,1,0:T(4,128)}, u32[]{:S(2)}) copy-start(f32[4,4,2048]{2,1,0:T(4,128)} %gate_ref.1) | copy-start | bytes 393220
  38.0 21.9 %copy-start.3 = (bf16[2048,128]{1,0:T(8,128)(2,1)S(1)}, bf16[2048,128]{1,0:T(8,128)(2,1)}, u32[]{:S(2)}) copy-start(bf16[2048,128]{1,0:T(8,128)(2,1)} %weight_ref.1) | copy-start | bytes 1572868
  60.4 6.6 %collective-permute-start = (bf16[4,128]{1,0:T(4,128)(2,1)S(1)}, bf16[4,128]{1,0:T(4,128)(2,1)S(1)}, u32[]{:S(2)}, u32[]{:S(2)}) collective-permute-start(bf16[4,128]{1,0:T(4,128)(2,1)S(1)} %finish.1), channel_id=1, source_target_pairs={{0,1},{1,0},{2,3},{3,2},{4,5},{5,4},{6,7},{7,6},{8,9},{9,8},{10,11... | collective-permute-start | bytes 3080 | tf_op jit(solution)/shard_map/ppermute | solution.py:298

commit v2 on v1

--- a/solution.py
+++ b/solution.py
@@ -12,6 +12,7 @@
 HEADS = 64
 KV_HEADS = 8
 HEAD = 64
+POSITIONS = 2048
 KV = ("kv_0", "kv_1")
 
 EPSILON = 1e-06
@@ -30,21 +31,75 @@
     return jnp.concatenate([part[:, :half], part[:, half:]], axis=0)
 
 
-def project_kernel(tokens_ref, gain_ref, query_ref, key_ref, value_ref, gate_ref, out_ref):
+def project_kernel(
+    tokens_hbm,
+    norm_gain_hbm,
+    query_hbm,
+    key_hbm,
+    value_hbm,
+    gate_hbm,
+    bias_hbm,
+    query_gain_hbm,
+    key_gain_hbm,
+    lengths_hbm,
+    out_ref,
+    small_ref,
+    tokens_ref,
+    norm_gain_ref,
+    query_ref,
+    key_ref,
+    value_ref,
+    gate_ref,
+    bias_ref,
+    query_gain_ref,
+    key_gain_ref,
+    lengths_ref,
+    arrived,
+):
+    kv_rank = lax.axis_index(KV)
+    columns = tokens_ref.shape[1]
+    mine = pl.ds(pl.multiple_of(kv_rank * columns, columns), columns)
+    pairs = [
+        (tokens_hbm, tokens_ref),
+        (norm_gain_hbm, norm_gain_ref),
+        (query_hbm, query_ref),
+        (key_hbm, key_ref),
+        (value_hbm, value_ref),
+        (gate_hbm.at[:, mine], gate_ref),
+        (bias_hbm, bias_ref),
+        (query_gain_hbm, query_gain_ref),
+        (key_gain_hbm, key_gain_ref),
+        (lengths_hbm, lengths_ref),
+    ]
+    copies = [pltpu.make_async_copy(*pair, arrived.at[k]) for k, pair in enumerate(pairs)]
+    for copy in copies:
+        copy.start()
+    for copy in copies:
+        copy.wait()
     tokens = tokens_ref[...].astype(F32)
     squares = jnp.sum(tokens * tokens, axis=1, keepdims=True)
-    scaled = (tokens * gain_ref[...]).astype(BF16)
+    scaled = (tokens * norm_gain_ref[...]).astype(BF16)
     query = jnp.dot(scaled, query_ref[...], preferred_element_type=F32)
     key = jnp.dot(scaled, key_ref[...], preferred_element_type=F32)
     value = jnp.dot(scaled, value_ref[...], preferred_element_type=F32)
-    gate = jnp.dot(scaled, gate_ref[...], preferred_element_type=F32)
-    extra = gate + jnp.where(lanes_of(gate.shape) == 4, squares, 0.0)
+    rows = jnp.concatenate([gate_ref[...].astype(F32), jnp.zeros((120, 128), F32)], axis=0)
+    gate = lax.dot_general(
+        scaled, rows.astype(BF16), (((1,), (1,)), ((), ())), preferred_element_type=F32
+    )
+    extra = gate + jnp.where(lanes_of(gate.shape) == KV_HEADS, squares, 0.0)
     extra = jnp.concatenate([extra, jnp.zeros_like(extra)], axis=0)
     whole = jnp.concatenate(
         [halves_stacked(query), halves_stacked(key), halves_stacked(value), extra], axis=1
     ).astype(BF16)
     for copy in range(out_ref.shape[0]):
         out_ref[copy] = whole
+    small_ref[0:1, :] = jnp.concatenate([query_gain_ref[...]] * 2, axis=1)
+    small_ref[1:2, :] = jnp.concatenate([key_gain_ref[...]] * 2, axis=1)
+    small_ref[2:3, :] = jnp.zeros((1, 128), F32)
+    small_ref[2:3, 0 : bias_ref.shape[1]] = bias_ref[...]
+    rest = lengths_ref[...] - kv_rank * POSITIONS
+    small_ref[3:4, :] = jnp.zeros((1, 128), F32)
+    small_ref[3:4, 0 : rest.shape[1]] = rest.astype(F32)
 
 
 def split_heads_sum(squares):
@@ -58,15 +113,33 @@
     )
 
 
+def fold_kernel(in_ref, out_ref):
+    total = in_ref[0].astype(F32)
+    for piece in range(1, in_ref.shape[0]):
+        total = total + in_ref[piece].astype(F32)
+    total = total.astype(BF16)
+    for copy in range(out_ref.shape[0]):
+        out_ref[copy] = total
+
+
 def attend_kernel(
-    rest_ref, sums_ref, small_ref, gate_ref, key_ref, value_ref, out_ref, query_ref
+    sums_ref,
+    small_ref,
+    gate_ref,
+    key_ref,
+    value_ref,
+    out_ref,
+    query_ref,
+    scores_ref,
+    weights_ref,
 ):
+    tp_rank = lax.axis_index("tp")
     seqs, positions = gate_ref.shape[0], gate_ref.shape[2]
     total = sums_ref[0].astype(F32)
     for piece in range(1, sums_ref.shape[0]):
         total = total + sums_ref[piece].astype(F32)
     extra = total[:, 1280:]
-    inverse = lax.rsqrt(extra[0:seqs, 4:5] / D + EPSILON)
+    inverse = lax.rsqrt(extra[0:seqs, KV_HEADS : KV_HEADS + 1] / D + EPSILON)
     inverse = jnp.concatenate([inverse, inverse], axis=0)
     raw = (total[:, :1280] * inverse).astype(BF16).astype(F32)
     tiles = [raw[:, 128 * k : 128 * (k + 1)] for k in range(10)]
@@ -80,63 +153,114 @@
     log_gate = jnp.minimum(logit, 0.0) - jnp.log1p(jnp.exp(-jnp.abs(logit)))
 
     lane = lanes_of((8, 128))
-    row = lax.broadcasted_iota(jnp.int32, (8, 128), 0)
-    left, early = lane < HEAD, row < 4
-    place = lanes_of((8, positions))
-    early_wide = lax.broadcasted_iota(jnp.int32, (8, positions), 0) < 4
-    maxima = jnp.zeros((8, 128), F32)
-    sums = jnp.zeros((8, 128), F32)
-    for s in range(seqs):
-        rest = rest_ref[s]
-        owner = jnp.logical_and(rest >= 1, rest <= positions)
-        live = place < rest
-        chosen = place == rest - 1
-        parts, gates, last, fresh = [], [], [], []
+    left = lane < HEAD
+    early = lax.broadcasted_iota(jnp.int32, (8, 128), 0) < 4
+    blocks = positions // 128
+    rest = [
+        jnp.broadcast_to(small_ref[3:4, s : s + 1], (8, 128)).astype(jnp.int32)
+        for s in range(seqs)
+    ]
+    owner = [jnp.logical_and(r >= 1, r <= positions) for r in rest]
+
+    def gate_rows(s, a, j):
+        part = slice(128 * j, 128 * j + 128)
+        return jnp.where(
+            early, gate_ref[s, 2 * a : 2 * a + 1, part], gate_ref[s, 2 * a + 1 : 2 * a + 2, part]
+        )
+
+    parts = {}
+    for s in range(seqs):
         for a in range(2):
             heads = query_ref[pl.ds(a * seqs + s, 8, stride=8), :]
             turned = pltpu.roll(heads, HEAD, 1)
             even = jnp.where(left == early, jnp.where(early, heads, turned), 0.0)
             odd = jnp.where(left == early, jnp.where(early, turned, heads), 0.0)
-            parts.append(jnp.concatenate([even, odd], axis=0) * HEAD ** (-0.5))
-            gate = jnp.where(
-                early_wide, gate_ref[s, 2 * a : 2 * a + 1, :], gate_ref[s, 2 * a + 1 : 2 * a + 2, :]
-            )
-            gates.append(gate)
-            own = jnp.sum(jnp.where(chosen, gate, 0.0), axis=1, keepdims=True)
-            wanted = jnp.where(early, 2 * a, 2 * a + 1)
-            own = own + jnp.sum(
-                jnp.where(lane == wanted, log_gate[s : s + 1, :], 0.0), axis=1, keepdims=True
-            )
-            new = jnp.sum(
-                parts[a] * keys_new[a * seqs + s : a * seqs + s + 1, :], axis=1, keepdims=True
-            )
-            fresh.append(new - jnp.concatenate([own, own], axis=0))
-        zeros = jnp.zeros((16, 128), F32)
+            parts[s, a, 0] = even * HEAD ** (-0.5)
+            parts[s, a, 1] = odd * HEAD ** (-0.5)
+    zeros = jnp.zeros((16, 128), F32)
+    for s in range(seqs):
         query = jnp.concatenate(
             [
-                jnp.concatenate([parts[0], zeros], axis=1),
-                jnp.concatenate([zeros, parts[1]], axis=1),
+                jnp.concatenate([parts[s, 0, 0], parts[s, 0, 1], zeros], axis=0),
+                jnp.concatenate([zeros, parts[s, 1, 0], parts[s, 1, 1]], axis=0),
             ],
-            axis=0,
+            axis=1,
         ).astype(BF16)
-        scores = lax.dot_general(
+        scores_ref[32 * s : 32 * s + 32, :] = lax.dot_general(
             query, key_ref[s], (((1,), (1,)), ((), ())), preferred_element_type=F32
         )
-        gate = jnp.concatenate([gates[0], gates[0], gates[1], gates[1]], axis=0)
-        live = jnp.concatenate([live] * 4, axis=0)
-        scores = jnp.where(live, scores - gate, FLOOR)
-        top = jnp.max(scores, axis=1, keepdims=True)
-        score_new = jnp.concatenate(fresh, axis=0)
-        top = jnp.where(owner, jnp.maximum(top, score_new), top)
-        weights = jnp.where(live, jnp.exp(scores - top), 0.0).astype(BF16)
-        weight_new = jnp.where(owner, jnp.exp(score_new - top), 0.0).astype(BF16).astype(F32)
-        count = jnp.sum(weights.astype(F32), axis=1, keepdims=True) + weight_new
-        summed = jnp.dot(weights, value_ref[s], preferred_element_type=F32)
+
+    tops, owns = {}, {}
+    for s in range(seqs):
         for a in range(2):
-            rows = slice(16 * a, 16 * a + 16)
-            mine = summed[rows, 128 * a : 128 * a + 128]
-            mine = mine + weight_new[rows] * values_new[a * seqs + s : a * seqs + s + 1, :]
-            even, odd = mine[:8], mine[8:]
+            tops[s, a, 0] = tops[s, a, 1] = jnp.full((8, 128), FLOOR, F32)
+            owns[s, a] = jnp.zeros((8, 128), F32)
+        for j in range(blocks):
+            place = lane + 128 * j
+            live, last = place < rest[s], place == rest[s] - 1
+            for a in range(2):
+                gate = gate_rows(s, a, j)
+                owns[s, a] = owns[s, a] + jnp.where(last, gate, 0.0)
+                for p in range(2):
+                    at = 32 * s + 16 * a + 8 * p
+                    score = scores_ref[at : at + 8, 128 * j : 128 * j + 128] - gate
+                    score = jnp.where(live, score, FLOOR)
+                    scores_ref[at : at + 8, 128 * j : 128 * j + 128] = score
+                    tops[s, a, p] = jnp.maximum(tops[s, a, p], score)
+    rows = [(s, a, p) for s in range(seqs) for a in range(2) for p in range(2)]
+    fresh, top, weight_new = {}, {}, {}
+    for s in range(seqs):
+        for a in range(2):
+            wanted = jnp.where(early, 2 * a, 2 * a + 1) + tp_rank * (KV_HEADS // 2)
+            own = owns[s, a] + jnp.where(lane == wanted, log_gate[s : s + 1, :], 0.0)
+            key_new = keys_new[a * seqs + s : a * seqs + s + 1, :]
+            for p in range(2):
+                fresh[s, a, p] = jnp.sum(parts[s, a, p] * key_new - own, axis=1, keepdims=True)
+    for s, a, p in rows:
+        most = jnp.max(tops[s, a, p], axis=1, keepdims=True)
+        new = jnp.broadcast_to(fresh[s, a, p], (8, 128))
+        most = jnp.broadcast_to(most, (8, 128))
+        top[s, a, p] = jnp.where(owner[s], jnp.maximum(most, new), most)
+        weight = jnp.where(owner[s], jnp.exp(new - top[s, a, p]), 0.0)
+        weight_new[s, a, p] = weight.astype(BF16).astype(F32)
+    counts = {}
+    for s in range(seqs):
+        for a in range(2):
+            counts[s, a, 0] = counts[s, a, 1] = jnp.zeros((8, 128), F32)
+        for j in range(blocks):
+            live = lane + 128 * j < rest[s]
+            for a in range(2):
+                both = []
+                for p in range(2):
+                    at = 32 * s + 16 * a + 8 * p
+                    score = scores_ref[at : at + 8, 128 * j : 128 * j + 128]
+                    weight = jnp.where(live, jnp.exp(score - top[s, a, p]), 0.0).astype(BF16)
+                    counts[s, a, p] = counts[s, a, p] + weight.astype(F32)
+                    both.append(weight)
+                at = 32 * s + 16 * a
+                weights_ref[at : at + 16, 128 * j : 128 * j + 128] = jnp.concatenate(both, axis=0)
+    summed = [
+        jnp.dot(
+            weights_ref[32 * s : 32 * s + 32, :], value_ref[s], preferred_element_type=F32
+        )
+        for s in range(seqs)
+    ]
+    maxima = jnp.zeros((8, 128), F32)
+    sums = jnp.zeros((8, 128), F32)
+    for s, a, p in rows:
+        here = lane == 4 * s + 2 * a + p
+        count = jnp.sum(counts[s, a, p], axis=1, keepdims=True) + weight_new[s, a, p]
+        maxima = jnp.where(here, top[s, a, p], maxima)
+        sums = jnp.where(here, count, sums)
+    packed = pack_statistics(maxima, sums)
+    for s in range(seqs):
+        for a in range(2):
+            new = values_new[a * seqs + s : a * seqs + s + 1, :]
+            even, odd = (
+                summed[s][16 * a + 8 * p : 16 * a + 8 * p + 8, 128 * a : 128 * a + 128]
+                + weight_new[s, a, p] * new
+                for p in range(2)
+            )
             dense = jnp.where(
                 left,
                 jnp.where(early, even, pltpu.roll(even, HEAD, 1)),
@@ -145,12 +269,6 @@
             at = 8 * (2 * s + a)
             for copy in range(out_ref.shape[0]):
                 out_ref[copy, at : at + 8, :] = dense
-            for p in range(2):
-                here = lane == 4 * s + 2 * a + p
-                own_rows = slice(16 * a + 8 * p, 16 * a + 8 * p + 8)
-                maxima = jnp.where(here, top[own_rows], maxima)
-                sums = jnp.where(here, count[own_rows], sums)
-    packed = pack_statistics(maxima, sums)
     for copy in range(out_ref.shape[0]):
         out_ref[copy, 64:72, :] = packed
 
@@ -221,6 +339,14 @@
 
 def in_vmem(count):
     return [pl.BlockSpec(memory_space=VMEM)] * count
+
+
+def in_hbm(count):
+    return [pl.BlockSpec(memory_space=pltpu.HBM)] * count
+
+
+def held(*arrays):
+    return [pltpu.with_memory_space_constraint(array, pltpu.HBM) for array in arrays]
 
 
 def exchanged(array, axis):
@@ -244,40 +370,68 @@
     out_weight,
 ):
     seqs, columns = tokens.shape
-    kv_rank = lax.axis_index(KV)
-    tp_rank = lax.axis_index("tp")
-    groups = key_weight.shape[1] // HEAD
-    positions = key_cache.shape[1]
     outer, inner = lax.axis_size("kv_0"), lax.axis_size("kv_1")
-    gate_rows = lax.dynamic_slice(
-        gate_weight, (kv_rank * columns, tp_rank * groups), (columns, groups)
-    )
-    gate_rows = jnp.pad(gate_rows, ((0, 0), (0, 128 - groups)))
-    local_bias = lax.dynamic_slice_in_dim(gate_bias, tp_rank * groups, groups)
-    small = jnp.stack(
-        [jnp.tile(query_gain, 2), jnp.tile(key_gain, 2), jnp.pad(local_bias, (0, 128 - groups))]
-    )
-    rest = lengths - kv_rank * positions
-
+    sums, small = pl.pallas_call(
+        project_kernel,
+        out_shape=(
+            jax.ShapeDtypeStruct((inner, 8, 1408), BF16),
+            jax.ShapeDtypeStruct((8, 128), F32),
+        ),
+        in_specs=in_hbm(10),
+        out_specs=tuple(in_vmem(2)),
+        scratch_shapes=[
+            VMEM(tokens.shape, BF16),
+            VMEM((1, columns), F32),
+            VMEM(query_weight.shape, BF16),
+            VMEM(key_weight.shape, BF16),
+            VMEM(value_weight.shape, BF16),
+            VMEM((KV_HEADS, columns), BF16),
+            VMEM((1, KV_HEADS), F32),
+            VMEM((1, HEAD), F32),
+            VMEM((1, HEAD), F32),
+            VMEM((1, seqs), jnp.int32),
+            pltpu.SemaphoreType.DMA((10,)),
+        ],
+        compiler_params=limit(4),
+        name="project",
+    )(
+        *held(
+            tokens,
+            norm_gain[None],
+            query_weight,
+            key_weight,
+            value_weight,
+            gate_weight.T,
+            gate_bias[None],
+            query_gain[None],
+            key_gain[None],
+            lengths[None],
+        )
+    )
     sums = pl.pallas_call(
-        project_kernel,
-        out_shape=jax.ShapeDtypeStruct((inner, 8, 1408), BF16),
-        in_specs=in_vmem(6),
+        fold_kernel,
+        out_shape=jax.ShapeDtypeStruct((outer, 8, 1408), BF16),
+        in_specs=in_vmem(1),
         out_specs=in_vmem(1)[0],
         compiler_params=limit(4),
-        name="project",
-    )(tokens, norm_gain[None], query_weight, key_weight, value_weight, gate_rows)
-    sums = exchanged(sums, "kv_1").astype(F32).sum(0).astype(BF16)
-    sums = exchanged(jnp.broadcast_to(sums[None], (outer, 8, 1408)), "kv_0")
+        cost_estimate=pl.CostEstimate(
+            flops=10**10, bytes_accessed=10**8, transcendentals=0
+        ),
+        name="fold",
+    )(exchanged(sums, "kv_1"))
     parts = pl.pallas_call(
         attend_kernel,
         out_shape=jax.ShapeDtypeStruct((inner, 72, 128), BF16),
-        in_specs=[pl.BlockSpec(memory_space=pltpu.SMEM)] + in_vmem(5),
+        in_specs=in_vmem(5),
         out_specs=in_vmem(1)[0],
-        scratch_shapes=[VMEM((64, 128), F32)],
+        scratch_shapes=[
+            VMEM((64, 128), F32),
+            VMEM((32 * seqs, POSITIONS), F32),
+            VMEM((32 * seqs, POSITIONS), BF16),
+        ],
         compiler_params=limit(24),
         name="attend",
-    )(rest, sums, small, gate_cache, key_cache, value_cache)
+    )(exchanged(sums, "kv_0"), small, gate_cache, key_cache, value_cache)
     parts = pl.pallas_call(
         merge_kernel,
         out_shape=jax.ShapeDtypeStruct((outer, 72, 128), BF16),

time: 68.2 us -> 55.6 us (0.82)
  blocking collectives: 17.4 us -> 43.4 us
  local copies, waits for them, and re-layouts: 13.1 us -> 0.02 us
  starting transfers between devices: 18.8 us -> 5.76 us
  waiting for transfers between devices: 11.1 us -> 0.82 us
  Pallas kernels: 5.92 us -> 4.73 us
    all_to_all x2 -> x4, blocking collectives: 17.4 us -> 43.4 us  [exchanged(): return lax.all_to_all(array, axis, 0, 0, tiled=True)]
    all_to_all x2 -> x0, starting transfers between devices: 13 us -> none  [exchanged(): return lax.all_to_all(array, axis, 0, 0, tiled=True)]
    all_to_all x2 -> x0, waiting for transfers between devices: 10.3 us -> none  [exchanged(): return lax.all_to_all(array, axis, 0, 0, tiled=True)]
    unnamed x19 -> x8, local copies, waits for them, and re-layouts: 9.47 us -> 0.02 us
    pallas_call x1, Pallas kernels: 4.26 us -> 2.51 us  [per_device(): pl.pallas_call(attend_kernel, out_shape=jax.ShapeDtypeStruct((inner, 72,...]
    another operation x5 -> x0, local copies, waits for them, and re-layouts: 1.48 us -> none  [the longest x1 0.66 us: per_device(): jnp.tile(query_gain, 2)]
    dynamic_slice x2 -> x0, local copies, waits for them, and re-layouts: 1.48 us -> none  [the longest x1 0.75 us: per_device(): lax.dynamic_slice(gate_weight, (kv_rank * columns, tp_rank * groups), (co...]
    broadcast_in_dim x1 -> x0, local copies, waits for them, and re-layouts: 0.68 us -> none  [per_device(): sums = exchanged(jnp.broadcast_to(sums[None], (outer, 8, 1408)), 'kv_0')]
  transfers between devices with their start and end apart: 3 -> 1, of which waited for: 3 -> 1; matrix products, arithmetic and copies ran while one was open for 4% -> 0% of each run, Pallas kernels for 0% -> 0%
where the time goes in v2:
time: 55.6 us; the launch traced here: 55.3 us
  blocking collectives  43.4 us (78%)
  starting transfers between devices  5.76 us (10%)
  Pallas kernels  4.73 us (9%)
  waiting for transfers between devices  0.82 us (1%)
  other arithmetic  0.57 us (1%)
    all_to_all x4, blocking collectives, exchanged(): return lax.all_to_all(array, axis, 0, 0, tiled=True)  43.4 us
    ppermute x1, starting transfers between devices, per_device(): other = lax.ppermute(mixed, 'tp', [(0, 1), (1, 0)])  5.76 us
    pallas_call x1, Pallas kernels, per_device(): pl.pallas_call(attend_kernel, out_shape=jax.ShapeDtypeStruct((inner, 72,...  2.51 us
    pallas_call x1, Pallas kernels, per_device(): pl.pallas_call(project_kernel, out_shape=(jax.ShapeDtypeStruct((inner, 8,...  1.38 us
  transfers between devices with their start and end apart: 1, of which 1 were waited for; matrix products, arithmetic and copies ran while one was open for 0% of the time, Pallas kernels for 0%

profile of v2, /device:TPU:1, one launch (start us, length us, event | category | flops | bytes accessed | tf_op | source)
XLA Modules:
  0.0 55.3 jit_solution(12426119396974082607)
XLA Ops:
  0.0 1.4 %project.1 = (bf16[4,8,1408]{2,1,0:T(8,128)(2,1)S(1)}, f32[8,128]{1,0:T(8,128)S(1)}) custom-call(bf16[4,128]{1,0:T(4,128)(2,1)} %tokens_hbm.1, f32[1,128]{1,0:T(1,128)} %bitcast.7, bf16[128,2048]{1,0:T(8,128)(2,1)} %query_hbm.1, bf16[128,256]{1,0:T(8,128)(2,1)} %key_hbm.1, bf16[128,256]{1,0:T(8,128)(2,1)} %value_hbm.1, bf16[8,4096]{1,0:T(8,128)(2,1)} %bitcast.6, ...), custom_call_target="tpu_custom_call" | custom-call | tf_op jit(solution)/shard_map/project/pallas_call | solution.py:374
  1.4 9.2 %all_to_all.20.in_ref = bf16[4,8,1408]{2,1,0:T(8,128)(2,1)S(1)} all-to-all(bf16[4,8,1408]{2,1,0:T(8,128)(2,1)S(1)} %get-tuple-element.7), channel_id=1, replica_groups=mesh['dp'=4,'kv_0'=8,'kv_1'=4,'tp'=2] {'kv_1'}, dimensions={0} | all-to-all | bytes 180224 | tf_op jit(solution)/shard_map/all_to_all | solution.py:353
  10.6 0.0 copy-start
  10.6 0.0 copy-start.1
  10.6 0.0 copy-start.3
  10.7 16.8 %all_to_all.21.sums_ref = bf16[8,8,1408]{2,1,0:T(8,128)(2,1)S(1)} all-to-all(bf16[8,8,1408]{2,1,0:T(8,128)(2,1)S(1)} %fold.1), channel_id=1, replica_groups=mesh['dp'=4,'kv_0'=8,'kv_1'=4,'tp'=2] {'kv_0'}, dimensions={0} | all-to-all | bytes 360448 | tf_op jit(solution)/shard_map/all_to_all | solution.py:353
  27.5 0.0 copy-done
  27.5 0.0 copy-done.1
  27.5 0.0 copy-done.3
  27.5 0.0 copy-start.2
  27.5 2.5 %attend.1 = bf16[4,72,128]{2,1,0:T(8,128)(2,1)S(1)} custom-call(bf16[8,8,1408]{2,1,0:T(8,128)(2,1)S(1)} %all_to_all.21.sums_ref, f32[8,128]{1,0:T(8,128)S(1)} %get-tuple-element.8.small_ref, f32[4,4,2048]{2,1,0:T(4,128)S(1)} %copy-done.3, bf16[4,2048,256]{2,1,0:T(8,128)(2,1)S(1)} %copy-done, bf16[4,2048,256]{2,1,0:T(8,128)(2,1)S(1)} %copy-done.1), custom_call_target="tpu_custom_call" | custom-call | tf_op jit(solution)/shard_map/attend/pallas_call | solution.py:422
  30.0 6.9 %all_to_all.22.in_ref = bf16[4,72,128]{2,1,0:T(8,128)(2,1)S(1)} all-to-all(bf16[4,72,128]{2,1,0:T(8,128)(2,1)S(1)} %attend.1), channel_id=1, replica_groups=mesh['dp'=4,'kv_0'=8,'kv_1'=4,'tp'=2] {'kv_1'}, dimensions={0} | all-to-all | bytes 147456 | tf_op jit(solution)/shard_map/all_to_all | solution.py:353
  36.9 0.3 merge.1
  37.2 10.5 %all_to_all.23.in_ref = bf16[8,72,128]{2,1,0:T(8,128)(2,1)S(1)} all-to-all(bf16[8,72,128]{2,1,0:T(8,128)(2,1)S(1)} %merge.1), channel_id=1, replica_groups=mesh['dp'=4,'kv_0'=8,'kv_1'=4,'tp'=2] {'kv_0'}, dimensions={0} | all-to-all | bytes 294912 | tf_op jit(solution)/shard_map/all_to_all | solution.py:353
  47.6 0.0 copy-done.2
  47.6 0.5 finish.1
  48.2 5.8 %collective-permute-start = (bf16[4,128]{1,0:T(4,128)(2,1)S(1)}, bf16[4,128]{1,0:T(4,128)(2,1)S(1)}, u32[]{:S(2)}, u32[]{:S(2)}) collective-permute-start(bf16[4,128]{1,0:T(4,128)(2,1)S(1)} %finish.1), channel_id=1, source_target_pairs={{0,1},{1,0},{2,3},{3,2},{4,5},{5,4},{6,7},{7,6},{8,9},{9,8},{10,11... | collective-permute-start | bytes 3080 | tf_op jit(solution)/shard_map/ppermute | solution.py:452
  54.0 0.8 %collective-permute-done = bf16[4,128]{1,0:T(4,128)(2,1)S(1)} collective-permute-done((bf16[4,128]{1,0:T(4,128)(2,1)S(1)}, bf16[4,128]{1,0:T(4,128)(2,1)S(1)}, u32[]{:S(2)}, u32[]{:S(2)}) %collective-permute-start) | collective-permute-done | bytes 1056 | tf_op jit(solution)/shard_map/ppermute | solution.py:452
  54.8 0.6 %add_convert_fusion = bf16[4,128]{1,0:T(4,128)(2,1)} fusion(bf16[4,128]{1,0:T(4,128)(2,1)S(1)} %collective-permute-done, bf16[4,128]{1,0:T(4,128)(2,1)S(1)} %finish.1), kind=kLoop, calls=%fused_computation | loop fusion | flops 2048 | bytes 3072 | tf_op jit(solution)/shard_map/convert_element_type | solution.py:453
  (1 shorter events, 0.0 us)
Async XLA Ops:
  10.6 16.8 %copy-start = (bf16[4,2048,256]{2,1,0:T(8,128)(2,1)S(1)}, bf16[4,2048,256]{2,1,0:T(8,128)(2,1)}, u32[]{:S(2)}) copy-start(bf16[4,2048,256]{2,1,0:T(8,128)(2,1)} %key_ref.1) | copy-start | bytes 12582916
  10.6 16.8 %copy-start.1 = (bf16[4,2048,256]{2,1,0:T(8,128)(2,1)S(1)}, bf16[4,2048,256]{2,1,0:T(8,128)(2,1)}, u32[]{:S(2)}) copy-start(bf16[4,2048,256]{2,1,0:T(8,128)(2,1)} %value_ref.1) | copy-start | bytes 12582916
  10.6 16.8 %copy-start.3 = (f32[4,4,2048]{2,1,0:T(4,128)S(1)}, f32[4,4,2048]{2,1,0:T(4,128)}, u32[]{:S(2)}) copy-start(f32[4,4,2048]{2,1,0:T(4,128)} %gate_ref.1) | copy-start | bytes 393220
  27.5 20.2 %copy-start.2 = (bf16[2048,128]{1,0:T(8,128)(2,1)S(1)}, bf16[2048,128]{1,0:T(8,128)(2,1)}, u32[]{:S(2)}) copy-start(bf16[2048,128]{1,0:T(8,128)(2,1)} %weight_ref.1) | copy-start | bytes 1572868
  48.2 6.6 %collective-permute-start = (bf16[4,128]{1,0:T(4,128)(2,1)S(1)}, bf16[4,128]{1,0:T(4,128)(2,1)S(1)}, u32[]{:S(2)}, u32[]{:S(2)}) collective-permute-start(bf16[4,128]{1,0:T(4,128)(2,1)S(1)} %finish.1), channel_id=1, source_target_pairs={{0,1},{1,0},{2,3},{3,2},{4,5},{5,4},{6,7},{7,6},{8,9},{9,8},{10,11... | collective-permute-start | bytes 3080 | tf_op jit(solution)/shard_map/ppermute | solution.py:452
